TPU v7x, 32 devices: a whole 2x2x4 slice. The times are simulated.
32 devices in a mesh: sp: 8 (over z, x), tp: 4 (over y, core).
Axes of the slice: x: 2, y: 2, z: 4, core: 2. Of those that a mesh axis runs over, the one named last changes fastest.
Arguments:
- residual: bfloat16 [1536, 2048], P('sp', 'tp'), may hold values from -10 to 10
- queries: bfloat16 [1536, 16, 128], P('sp', 'tp'), may hold values from -6.5 to 6.5
- key_rows: bfloat16 [1536, 16, 128], P('sp', 'tp'), may hold values from -6.5 to 6.5
- value_rows: bfloat16 [1536, 16, 128], P('sp', 'tp'), may hold values from -6 to 6
- diff_scale: float32 [16], P('tp'), may hold values from 0.3 to 0.8
- head_gain: float32 [128], replicated, may hold values from 0.1 to 1.9
- out_weight: bfloat16 [2048, 2048], P(None, 'tp'), may hold values from -0.125 to 0.125
- norm_gain: float32 [2048], replicated, may hold values from 0.1 to 1.9
- gate_weight: bfloat16 [8, 2048, 4096], P('sp', None, 'tp'), may hold values from -0.5 to 0.5
- up_weight: bfloat16 [8, 2048, 4096], P('sp', None, 'tp'), may hold values from -0.5 to 0.5
- down_weight: bfloat16 [8, 4096, 2048], P('sp', None, 'tp'), may hold values from -0.01171875 to 0.01171875
- expert_ids: int32 [1536, 2], P('sp'), may hold values from 0 to 7, all different within a row; in each aligned block of 192 rows (0 to 191, 192 to 383, ...) at most 96 rows name the same one
- route_logit: float32 [1536, 2], P('sp'), may hold values from -6 to 6
Outputs:
- updated: bfloat16 [1536, 2048], P('sp', 'tp')
Inputs may be any that keep to these rules, and one draw needn't show every extreme that they name: `expert_ids`: A token's 2 experts differ. The 192 tokens of one index of sp name one expert at most 96 times, a bound that some block reaches on some index.
All inputs are finite; a program needn't handle non-finite values.
Results may differ from a plain program's by a relative error of at most 0.014.
Values may be sent and summed in bfloat16 or wider, within the bound.
A program may use at most 64 MiB of HBM per device.

v0:
```python
import math
import jax
import jax.numpy as jnp
from jax import lax
from jax.sharding import PartitionSpec as P

D = 2048
QK = 64
SPAN = 64
NORM_EPS = 1e-05
CLAMP_LIMIT = 7.0
SWISH_ALPHA = 1.702
HEAD_KEEP = 0.8
NEG_FILL = -1e30


def update_map(running, query_half, key_half, value_block, visible):
    row_peak, row_total, accum = running
    scores = jnp.einsum(
        "qhd,khd->hqk", query_half, key_half, preferred_element_type=jnp.float32
    ) * QK ** (-0.5)
    scores = jnp.where(visible[None], scores, NEG_FILL)
    new_peak = jnp.maximum(row_peak, jnp.max(scores, axis=-1))
    exp_weights = jnp.where(visible[None], jnp.exp(scores - new_peak[..., None]), 0.0)
    rescale = jnp.exp(row_peak - new_peak)
    row_total = row_total * rescale + jnp.sum(exp_weights, axis=-1)
    accum = accum * rescale[..., None] + jnp.einsum(
        "hqk,khv->hqv",
        exp_weights.astype(jnp.bfloat16),
        value_block,
        preferred_element_type=jnp.float32,
    )
    return (new_peak, row_total, accum)


def local(
    residual,
    queries,
    key_rows,
    value_rows,
    diff_scale,
    head_gain,
    out_weight,
    norm_gain,
    gate_weight,
    up_weight,
    down_weight,
    expert_ids,
    route_logit,
):
    tokens_here = queries.shape[0]
    heads_here = queries.shape[1]
    value_width = value_rows.shape[2]
    query_start = lax.axis_index("sp") * tokens_here
    query_span = (query_start + jnp.arange(tokens_here, dtype=jnp.int32)) // SPAN
    first_query = queries[..., :QK]
    second_query = queries[..., QK:]
    empty_map = (
        jnp.full((heads_here, tokens_here), NEG_FILL, jnp.float32),
        jnp.zeros((heads_here, tokens_here), jnp.float32),
        jnp.zeros((heads_here, tokens_here, value_width), jnp.float32),
    )
    folded = (empty_map, empty_map)
    key_piece = lax.all_gather(key_rows, "sp", axis=0, tiled=True)
    value_piece = lax.all_gather(value_rows, "sp", axis=0, tiled=True)
    key_count = key_piece.shape[0]
    key_width = math.gcd(key_count, 1024)
    blocks = key_count // key_width
    key_blocks = key_piece.reshape(blocks, key_width, heads_here, 2 * QK)
    value_blocks = value_piece.reshape(blocks, key_width, heads_here, value_width)

    def advance(running, inputs):
        block_index, key_block, value_block = inputs
        key_start = block_index * key_width

        def compute(current):
            key_span = (key_start + jnp.arange(key_width, dtype=jnp.int32)) // SPAN
            visible = key_span[None, :] <= query_span[:, None]
            first = update_map(current[0], first_query, key_block[..., :QK], value_block, visible)
            second = update_map(current[1], second_query, key_block[..., QK:], value_block, visible)
            return (first, second)

        running = lax.cond(
            key_start < query_start + tokens_here, compute, lambda current: current, running
        )
        return (running, None)

    folded, _ = lax.scan(
        advance, folded, (jnp.arange(blocks, dtype=jnp.int32), key_blocks, value_blocks)
    )
    first_map, second_map = folded
    mixture = (
        first_map[2] / first_map[1][..., None]
        - diff_scale[:, None, None] * second_map[2] / second_map[1][..., None]
    )
    scale_back = lax.rsqrt(jnp.mean(mixture * mixture, axis=-1, keepdims=True) + NORM_EPS)
    attended = (mixture * scale_back * head_gain * HEAD_KEEP).astype(jnp.bfloat16)
    column_width = out_weight.shape[1]
    head_weight = out_weight.reshape(-1, value_width, column_width)
    weight_slice = head_weight
    projected = jnp.einsum(
        "htv,hvd->td",
        lax.all_gather(attended, "tp", axis=0, tiled=True),
        weight_slice,
        preferred_element_type=jnp.float32,
    )
    after_mixer = (residual.astype(jnp.float32) + projected).astype(jnp.bfloat16)
    mixer_float = after_mixer.astype(jnp.float32)
    partial_value = jnp.sum(mixer_float * mixer_float, axis=-1)
    square_total = lax.psum(partial_value, "tp")
    gain_slice = lax.dynamic_slice_in_dim(
        norm_gain, lax.axis_index("tp") * column_width, column_width, 0
    )
    normed = (mixer_float * lax.rsqrt(square_total / D + NORM_EPS)[:, None] * gain_slice).astype(
        jnp.bfloat16
    )
    experts = lax.axis_size("sp")
    top_count = expert_ids.shape[1]
    capacity = 2 * tokens_here * top_count // experts
    chosen = expert_ids.reshape(-1)
    onehot = (chosen[:, None] == jnp.arange(experts, dtype=jnp.int32)[None, :]).astype(jnp.int32)
    rank_in = jnp.sum(jnp.cumsum(onehot, axis=0) * onehot, axis=1) - 1
    slot_index = chosen * capacity + rank_in
    owner_row = (
        jnp.full((experts * capacity,), tokens_here, jnp.int32)
        .at[slot_index]
        .set(jnp.arange(tokens_here * top_count, dtype=jnp.int32) // top_count)
    )
    padded = jnp.concatenate([normed, jnp.zeros((1, normed.shape[1]), jnp.bfloat16)], axis=0)
    outgoing = padded[owner_row].reshape(experts, capacity, normed.shape[1])
    expert_input = lax.all_gather(
        lax.all_to_all(outgoing, "sp", split_axis=0, concat_axis=0, tiled=True),
        "tp",
        axis=2,
        tiled=True,
    )
    sources = expert_input.shape[0]
    items = expert_input.shape[1]
    flat_rows = expert_input.reshape(sources * items, -1)
    pre_gate = jnp.dot(flat_rows, gate_weight[0], preferred_element_type=jnp.float32)
    pre_up = jnp.dot(flat_rows, up_weight[0], preferred_element_type=jnp.float32)
    capped = jnp.minimum(pre_gate, CLAMP_LIMIT)
    linear = jnp.clip(pre_up, -CLAMP_LIMIT, CLAMP_LIMIT)
    hidden = (capped * jax.nn.sigmoid(SWISH_ALPHA * capped) * (linear + 1.0)).astype(jnp.bfloat16)
    weight_slice = down_weight[0]
    expert_out = jnp.dot(
        lax.all_gather(hidden, "tp", axis=1, tiled=True),
        weight_slice,
        preferred_element_type=jnp.float32,
    )
    expert_out = expert_out.astype(jnp.bfloat16).reshape(sources, items, -1)
    returned_rows = lax.all_to_all(expert_out, "sp", split_axis=0, concat_axis=0, tiled=True)
    picked = returned_rows.reshape(experts * capacity, -1)[slot_index].astype(jnp.float32)
    picked = picked.reshape(tokens_here, top_count, -1)
    weights = jax.nn.softmax(route_logit, axis=-1)
    routed = jnp.sum(picked * weights[..., None], axis=1)
    return (mixer_float + routed).astype(jnp.bfloat16)


def solution(mesh):
    return jax.shard_map(
        local,
        mesh=mesh,
        in_specs=(
            P("sp", "tp"),
            P("sp", "tp", None),
            P("sp", "tp", None),
            P("sp", "tp", None),
            P("tp"),
            P(),
            P(None, "tp"),
            P(),
            P("sp", None, "tp"),
            P("sp", None, "tp"),
            P("sp", None, "tp"),
            P("sp", None),
            P("sp", None),
        ),
        out_specs=P("sp", "tp"),
        check_vma=False,
    )
```

profile of v0, /device:TPU:0, one launch (start us, length us, event | category | flops | bytes accessed | tf_op | source)
XLA Modules:
  0.0 296.3 jit_solution(3500172858010482587)
XLA Ops:
  6.5 1.8 copy.27
  8.4 1.6 copy.29
  10.1 0.8 copy.34
  11.8 0.9 reduce-window.6
  13.2 0.8 dynamic_slice.28
  14.1 2.9 scatter_custom_fusion
  17.0 39.5 %all-gather.5.cloned.1.call-done = bf16[1536,4,128]{2,0,1:T(8,128)(2,1)} async-done(((bf16[192,4,128]{2,0,1:T(8,128)(2,1)}), bf16[1536,4,128]{2,0,1:T(8,128)(2,1)}) %all-gather.5.cloned.1.call-update) | async-done | bytes 1572880 | tf_op jit(solution)/shard_map/all_gather | solution.py:64
  56.5 2.6 copy.31
  59.1 42.2 %all-gather.7.cloned.1.call-done = bf16[1536,4,128]{2,0,1:T(8,128)(2,1)} async-done(((bf16[192,4,128]{2,0,1:T(8,128)(2,1)}), bf16[1536,4,128]{2,0,1:T(8,128)(2,1)}) %all-gather.7.cloned.1.call-update) | async-done | bytes 1572880 | tf_op jit(solution)/shard_map/all_gather | solution.py:65
  101.2 2.7 copy.32
  104.0 9.0 %while.23 = (s32[]{:T(128)}, f32[4,192]{1,0:T(4,128)S(1)}, f32[4,192]{1,0:T(4,128)S(1)}, f32[4,192,128]{2,1,0:T(8,128)S(1)}, f32[4,192]{1,0:T(4,128)S(1)}, /*ind...) while((s32[]{:T(128)}, f32[4,192]{1,0:T(4,128)S(1)}, ...), condition=%wide.region_7.8_spmd.clone, body=%wide.region_0.7_spmd.clone.sunk | while | flops 309574784 | bytes 20891532 | solution.py:88
  104.1 0.6 dynamic_slice.42
  105.4 5.0 %conditional.3 = ((f32[4,192]{1,0:T(4,128)S(1)}, f32[4,192]{1,0:T(4,128)S(1)}, f32[4,192,128]{2,1,0:T(8,128)S(1)}, f32[4,192]{1,0:T(4,128)S(1)}, f32[4,192]{1,0:T(4,128)S(1)}, /*index=5*/f32[4,192,128]{2,1,0:T(8,128)S(1)})) conditional(s32[]{:T(128)} %convert_element_type.82, (f32[4,192]{1,0:T(4,128)S(1)}, f32[4,192]{1,0:T(4,128)S(1)}, ...), branch_computations={%region_1.1_spmd, %region_2.6_spmd.clone} | conditional | flops 309572096 | bytes 20887848 | solution.py:83
  105.5 1.1 dynamic-slice_bitcast_fusion
  107.8 1.2 fusion.5
  110.4 0.6 dynamic_slice.42
  113.7 8.6 %all_gather.17 = bf16[16,192,128]{2,1,0:T(8,128)(2,1)S(1)} all-gather(bf16[4,192,128]{2,1,0:T(8,128)(2,1)S(1)} %multiply_convert_fusion.2), channel_id=1, replica_groups=mesh['sp'=8,'tp'=4] {'tp'}, dimensions={0}, use_global_device_ids=true | all-gather | bytes 983040 | tf_op jit(solution)/shard_map/all_gather | solution.py:103
  122.3 0.7 multiply_reduce_fusion.1
  123.0 6.2 %psum.7 = f32[192]{0:T(256)S(1)} all-reduce(f32[192]{0:T(256)S(1)} %get-tuple-element.467), channel_id=1, replica_groups=mesh['sp'=8,'tp'=4] {'tp'}, use_global_device_ids=true, to_apply=%region_10.11 | all-reduce | flops 192 | bytes 1536 | tf_op jit(solution)/shard_map/psum | solution.py:110
  129.3 2.7 gather_fusion
  132.0 32.5 %all_to_all.10 = bf16[8,96,512]{2,1,0:T(8,128)(2,1)} all-to-all(bf16[8,96,512]{2,1,0:T(8,128)(2,1)S(1)} %bitcast.62), channel_id=1, replica_groups=mesh['sp'=8,'tp'=4] {'sp'}, dimensions={0} | all-to-all | bytes 1572864 | tf_op jit(solution)/shard_map/all_to_all | solution.py:132
  164.7 26.5 %all-gather.9.cloned.1.call-done = bf16[8,96,2048]{2,1,0:T(8,128)(2,1)} async-done(((bf16[8,96,512]{2,1,0:T(8,128)(2,1)}), bf16[8,96,2048]{2,1,0:T(8,128)(2,1)}) %all-gather.9.cloned.1.call-update) | async-done | bytes 3145744 | tf_op jit(solution)/shard_map/all_gather | solution.py:131
  191.3 6.3 %fusion.32 = f32[768,1024]{1,0:T(8,128)S(1)} fusion(bf16[768,2048]{1,0:T(8,128)(2,1)} %bitcast.67, bf16[1,2048,1024]{2,1,0:T(8,128)(2,1)} %param.26), kind=kOutput, calls=%fused_computation.55 | convolution fusion | flops 3221225472 | bytes 10485760 | tf_op jit(solution)/shard_map/dot_general | solution.py:141
  197.6 5.3 %multiply_convert_fusion = bf16[768,1024]{1,0:T(8,128)(2,1)} fusion(f32[768,1024]{1,0:T(8,128)S(1)} %fusion.32, bf16[768,2048]{1,0:T(8,128)(2,1)S(1)} %bitcast.68, bf16[1,2048,1024]{2,1,0:T(8,128)(2,1)S(1)} %copy-done.8), kind=kOutput, calls=%fused_computation.59 | convolution fusion | flops 3229089792 | bytes 12058624 | tf_op jit(solution)/shard_map/dot_general | solution.py:140
  202.9 46.5 %all-gather.11.cloned.1.call-done = bf16[768,4096]{1,0:T(8,128)(2,1)} async-done(((bf16[768,1024]{1,0:T(8,128)(2,1)}), bf16[768,4096]{1,0:T(8,128)(2,1)}) %all-gather.11.cloned.1.call-update) | async-done | bytes 6291472 | tf_op jit(solution)/shard_map/all_gather | solution.py:147
  249.4 8.3 %fusion.38 = bf16[768,512]{1,0:T(8,128)(2,1)} fusion(bf16[768,4096]{1,0:T(8,128)(2,1)} %all-gather.11.cloned.1.call-done, bf16[1,4096,512]{2,1,0:T(8,128)(2,1)} %param.27), kind=kOutput, calls=%fused_computation.60 | convolution fusion | flops 3221618688 | bytes 11272192 | tf_op jit(solution)/shard_map/dot_general | solution.py:146
  257.7 5.6 %all-to-all-start.1 = ((bf16[8,96,512]{2,1,0:T(8,128)(2,1)}), bf16[8,96,512]{2,1,0:T(8,128)(2,1)S(1)}, u32[]{:S(2)}, u32[]{:S(2)}) async-start(bf16[8,96,512]{2,1,0:T(8,128)(2,1)} %bitcast.65), calls=%async_computation.1 | async-start | bytes 1572864 | tf_op jit(solution)/shard_map/all_to_all | solution.py:152
  263.6 20.4 %all-to-all-done.1 = bf16[8,96,512]{2,1,0:T(8,128)(2,1)S(1)} async-done(((bf16[8,96,512]{2,1,0:T(8,128)(2,1)}), bf16[8,96,512]{2,1,0:T(8,128)(2,1)S(1)}, u32[]{:S(2)}, u32[]{:S(2)}) %all-to-all-start.1) | async-done | bytes 786464 | tf_op jit(solution)/shard_map/all_to_all | solution.py:152
  283.9 2.6 gather_fusion.1
  286.5 1.5 reshape.153
  288.0 1.0 multiply_reduce_fusion
  289.0 0.7 add_convert_fusion
  (90 shorter events, 6.2 us)
Async XLA Ops:
  6.5 115.8 %copy-start = (bf16[2048,512]{1,0:T(8,128)(2,1)S(1)}, bf16[2048,512]{1,0:T(8,128)(2,1)}, u32[]{:S(2)}) copy-start(bf16[2048,512]{1,0:T(8,128)(2,1)} %param.23) | copy-start | bytes 6291460
  6.5 6.4 %copy-start.5 = (s32[192,2]{0,1:T(2,128)S(1)}, s32[192,2]{0,1:T(2,128)}, u32[]{:S(2)}) copy-start(s32[192,2]{0,1:T(2,128)} %param.28) | copy-start | bytes 4612
  6.5 4.7 %copy-start.2 = (bf16[192,4,128]{2,1,0:T(4,128)(2,1)S(1)}, bf16[192,4,128]{2,1,0:T(4,128)(2,1)}, u32[]{:S(2)}) copy-start(bf16[192,4,128]{2,1,0:T(4,128)(2,1)} %param.18) | copy-start | bytes 589828
  6.5 49.9 %all-gather.5.cloned.1.call-start = ((), (), s32[]{:S(2)}) async-start(), calls=%async_computation.2 | async-start | bytes 1769472 | tf_op jit(solution)/shard_map/all_gather | solution.py:64
  8.4 92.9 %all-gather.7.cloned.1.call-start = ((), (), s32[]{:S(2)}) async-start(), calls=%async_computation.3 | async-start | bytes 1769472 | tf_op jit(solution)/shard_map/all_gather | solution.py:65
  10.1 181.2 %all-gather.9.cloned.1.call-start = ((), (), s32[]{:S(2)}) async-start(), calls=%async_computation.4 | async-start | bytes 3932160 | tf_op jit(solution)/shard_map/all_gather | solution.py:131
  104.0 9.0 %copy-start.6 = (f32[4]{0:T(128)S(1)}, f32[4]{0:T(128)}, u32[]{:S(2)}) copy-start(f32[4]{0:T(128)} %param.21) | copy-start | bytes 52
  104.0 9.5 %copy-start.7 = (f32[128]{0:T(128)S(1)}, f32[128]{0:T(128)}, u32[]{:S(2)}) copy-start(f32[128]{0:T(128)} %param.22) | copy-start | bytes 1540
  107.8 1.4 copy-start.1
  113.0 9.3 %copy-start.3 = (bf16[192,512]{1,0:T(8,128)(2,1)S(1)}, bf16[192,512]{1,0:T(8,128)(2,1)}, u32[]{:S(2)}) copy-start(bf16[192,512]{1,0:T(8,128)(2,1)} %param.17) | copy-start | bytes 589828
  164.5 84.9 %all-gather.11.cloned.1.call-start = ((), (), s32[]{:S(2)}) async-start(), calls=%async_computation.5 | async-start | bytes 7864320 | tf_op jit(solution)/shard_map/all_gather | solution.py:147
  191.2 6.3 %copy-start.8 = (bf16[1,2048,1024]{2,1,0:T(8,128)(2,1)S(1)}, bf16[1,2048,1024]{2,1,0:T(8,128)(2,1)}, u32[]{:S(2)}) copy-start(bf16[1,2048,1024]{2,1,0:T(8,128)(2,1)} %param.25) | copy-start | bytes 12582916
  191.3 6.3 %copy-start.9 = (bf16[8,96,2048]{2,1,0:T(8,128)(2,1)S(1)}, bf16[8,96,2048]{2,1,0:T(8,128)(2,1)}, u32[]{:S(2)}) copy-start(bf16[8,96,2048]{2,1,0:T(8,128)(2,1)} %all-gather.9.cloned.1.call-done) | copy-start | bytes 9437188
  257.7 5.7 %copy-start.4 = (f32[192,2]{0,1:T(2,128)S(1)}, f32[192,2]{0,1:T(2,128)}, u32[]{:S(2)}) copy-start(f32[192,2]{0,1:T(2,128)} %param.29) | copy-start | bytes 4612
  257.7 26.2 %all-to-all-start.1 = ((bf16[8,96,512]{2,1,0:T(8,128)(2,1)}), bf16[8,96,512]{2,1,0:T(8,128)(2,1)S(1)}, u32[]{:S(2)}, u32[]{:S(2)}) async-start(bf16[8,96,512]{2,1,0:T(8,128)(2,1)} %bitcast.65), calls=%async_computation.1 | async-start | bytes 1572864 | tf_op jit(solution)/shard_map/all_to_all | solution.py:152
Sparse Core Ops, SparseCore 0:
  9.5 46.9 all-gather.4
  58.7 42.5 all-gather.6
  164.6 26.5 all-gather.8
  203.0 46.3 all-gather.10
where the time goes:
time: 297 us; the launch traced here: 296 us
  waiting for transfers between devices  175 us (59%)
  blocking collectives  47.2 us (16%)
  local copies, waits for them, and re-layouts  24.5 us (8%)
  matrix products  22.8 us (8%)
  between operations  13.4 us (5%)
  starting transfers between devices  5.96 us (2%)
  other arithmetic  5.09 us (2%)
    all_gather x1, waiting for transfers between devices, local(): lax.all_gather(hidden, 'tp', axis=1, tiled=True)  46.5 us
    all_gather x1, waiting for transfers between devices, local(): value_piece = lax.all_gather(value_rows, 'sp', axis=0, tiled=True)  42.2 us
    all_gather x1, waiting for transfers between devices, local(): key_piece = lax.all_gather(key_rows, 'sp', axis=0, tiled=True)  39.5 us
    all_to_all x1, blocking collectives, local(): lax.all_to_all(outgoing, 'sp', split_axis=0, concat_axis=0, tiled=True)  32.5 us
    all_gather x1, waiting for transfers between devices, local(): lax.all_gather(lax.all_to_all(outgoing, 'sp', split_axis=0, concat_axis=0...  26.5 us
    all_to_all x1, waiting for transfers between devices, local(): lax.all_to_all(expert_out, 'sp', split_axis=0, concat_axis=0, tiled=True)  20.4 us
    unnamed x25, local copies, waits for them, and re-layouts  9.82 us
    all_gather x1, blocking collectives, local(): lax.all_gather(attended, 'tp', axis=0, tiled=True)  8.58 us
  transfers between devices with their start and end apart: 5, of which 5 were waited for; matrix products, arithmetic and copies ran while one was open for 4% of the time, Pallas kernels for 0%

commit v1 on v0

--- a/solution.py
+++ b/solution.py
@@ -61,8 +61,11 @@
         jnp.zeros((heads_here, tokens_here, value_width), jnp.float32),
     )
     folded = (empty_map, empty_map)
-    key_piece = lax.all_gather(key_rows, "sp", axis=0, tiled=True)
-    value_piece = lax.all_gather(value_rows, "sp", axis=0, tiled=True)
+    key_piece, value_piece = jnp.split(
+        lax.all_gather(jnp.concatenate([key_rows, value_rows], axis=1), "sp", axis=0, tiled=True),
+        [key_rows.shape[1]],
+        axis=1,
+    )
     key_count = key_piece.shape[0]
     key_width = math.gcd(key_count, 1024)
     blocks = key_count // key_width

time: 297 us -> 276 us (0.929)
  waiting for transfers between devices: 175 us -> 150 us
    all_gather x2 -> x1, waiting for transfers between devices: 81.6 us -> 56.6 us  [local(): lax.all_gather(jnp.concatenate([key_rows, value_rows], axis=1), 'sp', axi...]
    split x0 -> x1, local copies, waits for them, and re-layouts: none -> 3.81 us  [local(): jnp.split(lax.all_gather(jnp.concatenate([key_rows, value_rows], axis=1),...]
  transfers between devices with their start and end apart: 5 -> 4, of which waited for: 5 -> 4; matrix products, arithmetic and copies ran while one was open for 4% -> 2% of each run, Pallas kernels for 0% -> 0%
where the time goes in v1:
time: 276 us; the launch traced here: 275 us
  waiting for transfers between devices  150 us (54%)
  blocking collectives  47.8 us (17%)
  local copies, waits for them, and re-layouts  26.9 us (10%)
  matrix products  22.8 us (8%)
  between operations  13.4 us (5%)
  starting transfers between devices  5.9 us (2%)
  other arithmetic  5.87 us (2%)
    all_gather x1, waiting for transfers between devices, local(): lax.all_gather(jnp.concatenate([key_rows, value_rows], axis=1), 'sp', axi...  56.6 us
    all_gather x1, waiting for transfers between devices, local(): lax.all_gather(hidden, 'tp', axis=1, tiled=True)  46.5 us
    all_to_all x1, blocking collectives, local(): lax.all_to_all(outgoing, 'sp', split_axis=0, concat_axis=0, tiled=True)  33 us
    all_gather x1, waiting for transfers between devices, local(): lax.all_gather(lax.all_to_all(outgoing, 'sp', split_axis=0, concat_axis=0...  26.8 us
    all_to_all x1, waiting for transfers between devices, local(): lax.all_to_all(expert_out, 'sp', split_axis=0, concat_axis=0, tiled=True)  20.4 us
    all_gather x1, blocking collectives, local(): lax.all_gather(attended, 'tp', axis=0, tiled=True)  8.58 us
    dot_general x1, matrix products, local(): jnp.dot(lax.all_gather(hidden, 'tp', axis=1, tiled=True), weight_slice, p...  8.3 us
    unnamed x25, local copies, waits for them, and re-layouts  7.76 us
  transfers between devices with their start and end apart: 4, of which 4 were waited for; matrix products, arithmetic and copies ran while one was open for 2% of the time, Pallas kernels for 0%

profile of v1, /device:TPU:0, one launch (start us, length us, event | category | flops | bytes accessed | tf_op | source)
XLA Modules:
  0.0 275.1 jit_solution(14690558845845546398)
XLA Ops:
  6.5 1.1 copy.27
  7.7 1.0 copy.28
  8.6 0.8 pad_maximum_fusion
  10.4 0.9 reduce-window.6
  11.8 0.8 dynamic_slice.28
  12.7 2.9 %scatter_custom_fusion = s32[768]{0:T(1024)S(1)} fusion(s32[384]{0:T(512)S(1)} %fusion.51, s32[384]{0:T(512)S(1)} %add_select_fusion.1, s32[]{:T(128)} %constant.140.clone.1), kind=kCustom, calls=%fused_computation.91 | custom fusion | bytes 3076 | tf_op jit(solution)/shard_map/scatter | solution.py:130
  15.7 56.6 %all-gather.4.cloned.1.call-done = bf16[1536,8,128]{2,0,1:T(8,128)(2,1)} async-done(((bf16[192,8,128]{2,0,1:T(8,128)(2,1)}), bf16[1536,8,128]{2,0,1:T(8,128)(2,1)}) %all-gather.4.cloned.1.call-update) | async-done | bytes 3145744 | tf_op jit(solution)/shard_map/all_gather | solution.py:65
  72.3 3.8 %fusion.56 = (bf16[1536,4,128]{2,0,1:T(8,128)(2,1)}, bf16[1536,4,128]{2,0,1:T(8,128)(2,1)}) fusion(bf16[1536,8,128]{2,0,1:T(8,128)(2,1)} %all-gather.4.cloned.1.call-done), kind=kLoop, calls=%fused_computation.102 | loop fusion | bytes 6291456 | tf_op jit(solution)/shard_map/split | solution.py:64
  76.1 2.6 copy.31
  78.7 2.7 copy.32
  81.5 8.9 %while.23 = (s32[]{:T(128)}, f32[4,192]{1,0:T(4,128)S(1)}, f32[4,192]{1,0:T(4,128)S(1)}, f32[4,192,128]{2,1,0:T(8,128)S(1)}, f32[4,192]{1,0:T(4,128)S(1)}, /*ind...) while((s32[]{:T(128)}, f32[4,192]{1,0:T(4,128)S(1)}, ...), condition=%wide.region_7.8_spmd.clone, body=%wide.region_0.7_spmd.clone.sunk | while | flops 309574784 | bytes 20891532 | solution.py:91
  81.5 0.6 dynamic_slice.42
  82.8 5.0 %conditional.3 = ((f32[4,192]{1,0:T(4,128)S(1)}, f32[4,192]{1,0:T(4,128)S(1)}, f32[4,192,128]{2,1,0:T(8,128)S(1)}, f32[4,192]{1,0:T(4,128)S(1)}, f32[4,192]{1,0:T(4,128)S(1)}, /*index=5*/f32[4,192,128]{2,1,0:T(8,128)S(1)})) conditional(s32[]{:T(128)} %convert_element_type.82, (f32[4,192]{1,0:T(4,128)S(1)}, f32[4,192]{1,0:T(4,128)S(1)}, ...), branch_computations={%region_1.1_spmd, %region_2.6_spmd.clone} | conditional | flops 309572096 | bytes 20887848 | solution.py:86
  83.0 1.1 dynamic-slice_bitcast_fusion
  85.2 1.2 fusion.5
  87.8 0.6 dynamic_slice.42
  91.2 8.6 %all_gather.13 = bf16[16,192,128]{2,1,0:T(8,128)(2,1)S(1)} all-gather(bf16[4,192,128]{2,1,0:T(8,128)(2,1)S(1)} %multiply_convert_fusion.2), channel_id=1, replica_groups=mesh['sp'=8,'tp'=4] {'tp'}, dimensions={0}, use_global_device_ids=true | all-gather | bytes 983040 | tf_op jit(solution)/shard_map/all_gather | solution.py:106
  99.8 0.7 multiply_reduce_fusion.1
  100.4 6.2 %psum.7 = f32[192]{0:T(256)S(1)} all-reduce(f32[192]{0:T(256)S(1)} %get-tuple-element.469), channel_id=1, replica_groups=mesh['sp'=8,'tp'=4] {'tp'}, use_global_device_ids=true, to_apply=%region_10.11 | all-reduce | flops 192 | bytes 1536 | tf_op jit(solution)/shard_map/psum | solution.py:113
  106.7 3.3 %gather_fusion = bf16[768,512]{1,0:T(8,128)(2,1)} fusion(bf16[193,512]{1,0:T(8,128)(2,1)S(1)} %concatenate.7, s32[1024]{0:T(1024)S(1)} %pad_clamp_fusion.1), kind=kCustom, calls=%fused_computation | custom fusion | bytes 1575936 | tf_op jit(solution)/shard_map/gather | solution.py:133
  110.1 33.0 %all_to_all.10 = bf16[8,96,512]{2,1,0:T(8,128)(2,1)} all-to-all(bf16[8,96,512]{2,1,0:T(8,128)(2,1)} %bitcast.64), channel_id=1, replica_groups=mesh['sp'=8,'tp'=4] {'sp'}, dimensions={0} | all-to-all | bytes 1572864 | tf_op jit(solution)/shard_map/all_to_all | solution.py:135
  143.4 26.8 %all-gather.6.cloned.1.call-done = bf16[8,96,2048]{2,1,0:T(8,128)(2,1)} async-done(((bf16[8,96,512]{2,1,0:T(8,128)(2,1)}), bf16[8,96,2048]{2,1,0:T(8,128)(2,1)}) %all-gather.6.cloned.1.call-update) | async-done | bytes 3145744 | tf_op jit(solution)/shard_map/all_gather | solution.py:134
  170.1 6.3 %fusion.32 = f32[768,1024]{1,0:T(8,128)S(1)} fusion(bf16[768,2048]{1,0:T(8,128)(2,1)} %bitcast.67, bf16[1,2048,1024]{2,1,0:T(8,128)(2,1)} %param.26), kind=kOutput, calls=%fused_computation.55 | convolution fusion | flops 3221225472 | bytes 10485760 | tf_op jit(solution)/shard_map/dot_general | solution.py:144
  176.4 5.3 %multiply_convert_fusion = bf16[768,1024]{1,0:T(8,128)(2,1)} fusion(f32[768,1024]{1,0:T(8,128)S(1)} %fusion.32, bf16[768,2048]{1,0:T(8,128)(2,1)S(1)} %bitcast.68, bf16[1,2048,1024]{2,1,0:T(8,128)(2,1)S(1)} %copy-done.8), kind=kOutput, calls=%fused_computation.59 | convolution fusion | flops 3229089792 | bytes 12058624 | tf_op jit(solution)/shard_map/dot_general | solution.py:143
  181.8 46.5 %all-gather.8.cloned.1.call-done = bf16[768,4096]{1,0:T(8,128)(2,1)} async-done(((bf16[768,1024]{1,0:T(8,128)(2,1)}), bf16[768,4096]{1,0:T(8,128)(2,1)}) %all-gather.8.cloned.1.call-update) | async-done | bytes 6291472 | tf_op jit(solution)/shard_map/all_gather | solution.py:150
  228.3 8.3 %fusion.38 = bf16[768,512]{1,0:T(8,128)(2,1)} fusion(bf16[768,4096]{1,0:T(8,128)(2,1)} %all-gather.8.cloned.1.call-done, bf16[1,4096,512]{2,1,0:T(8,128)(2,1)} %param.27), kind=kOutput, calls=%fused_computation.60 | convolution fusion | flops 3221618688 | bytes 11272192 | tf_op jit(solution)/shard_map/dot_general | solution.py:149
  236.6 5.6 %all-to-all-start.1 = ((bf16[8,96,512]{2,1,0:T(8,128)(2,1)}), bf16[8,96,512]{2,1,0:T(8,128)(2,1)S(1)}, u32[]{:S(2)}, u32[]{:S(2)}) async-start(bf16[8,96,512]{2,1,0:T(8,128)(2,1)} %bitcast.65), calls=%async_computation.1 | async-start | bytes 1572864 | tf_op jit(solution)/shard_map/all_to_all | solution.py:155
  242.4 20.4 %all-to-all-done.1 = bf16[8,96,512]{2,1,0:T(8,128)(2,1)S(1)} async-done(((bf16[8,96,512]{2,1,0:T(8,128)(2,1)}), bf16[8,96,512]{2,1,0:T(8,128)(2,1)S(1)}, u32[]{:S(2)}, u32[]{:S(2)}) %all-to-all-start.1) | async-done | bytes 786464 | tf_op jit(solution)/shard_map/all_to_all | solution.py:155
  262.8 2.6 gather_fusion.1
  265.4 1.5 reshape.153
  266.9 1.0 multiply_reduce_fusion
  267.9 0.7 add_convert_fusion
  (89 shorter events, 6.3 us)
Async XLA Ops:
  6.5 93.2 %copy-start = (bf16[2048,512]{1,0:T(8,128)(2,1)S(1)}, bf16[2048,512]{1,0:T(8,128)(2,1)}, u32[]{:S(2)}) copy-start(bf16[2048,512]{1,0:T(8,128)(2,1)} %param.23) | copy-start | bytes 6291460
  6.5 2.9 %copy-start.5 = (s32[192,2]{0,1:T(2,128)S(1)}, s32[192,2]{0,1:T(2,128)}, u32[]{:S(2)}) copy-start(s32[192,2]{0,1:T(2,128)} %param.28) | copy-start | bytes 4612
  6.5 3.4 %copy-start.2 = (bf16[192,4,128]{2,1,0:T(4,128)(2,1)S(1)}, bf16[192,4,128]{2,1,0:T(4,128)(2,1)}, u32[]{:S(2)}) copy-start(bf16[192,4,128]{2,1,0:T(4,128)(2,1)} %param.18) | copy-start | bytes 589828
  6.5 65.8 %all-gather.4.cloned.1.call-start = ((), (), s32[]{:S(2)}) async-start(), calls=%async_computation.2 | async-start | bytes 3538944 | tf_op jit(solution)/shard_map/all_gather | solution.py:65
  9.4 160.7 %all-gather.6.cloned.1.call-start = ((), (), s32[]{:S(2)}) async-start(), calls=%async_computation.3 | async-start | bytes 3932160 | tf_op jit(solution)/shard_map/all_gather | solution.py:134
  81.5 9.0 %copy-start.6 = (f32[4]{0:T(128)S(1)}, f32[4]{0:T(128)}, u32[]{:S(2)}) copy-start(f32[4]{0:T(128)} %param.21) | copy-start | bytes 52
  81.5 9.5 %copy-start.7 = (f32[128]{0:T(128)S(1)}, f32[128]{0:T(128)}, u32[]{:S(2)}) copy-start(f32[128]{0:T(128)} %param.22) | copy-start | bytes 1540
  85.2 1.4 copy-start.1
  90.5 9.3 %copy-start.3 = (bf16[192,512]{1,0:T(8,128)(2,1)S(1)}, bf16[192,512]{1,0:T(8,128)(2,1)}, u32[]{:S(2)}) copy-start(bf16[192,512]{1,0:T(8,128)(2,1)} %param.17) | copy-start | bytes 589828
  143.1 85.2 %all-gather.8.cloned.1.call-start = ((), (), s32[]{:S(2)}) async-start(), calls=%async_computation.4 | async-start | bytes 7864320 | tf_op jit(solution)/shard_map/all_gather | solution.py:150
  170.1 6.3 %copy-start.8 = (bf16[1,2048,1024]{2,1,0:T(8,128)(2,1)S(1)}, bf16[1,2048,1024]{2,1,0:T(8,128)(2,1)}, u32[]{:S(2)}) copy-start(bf16[1,2048,1024]{2,1,0:T(8,128)(2,1)} %param.25) | copy-start | bytes 12582916
  170.1 6.3 %copy-start.9 = (bf16[8,96,2048]{2,1,0:T(8,128)(2,1)S(1)}, bf16[8,96,2048]{2,1,0:T(8,128)(2,1)}, u32[]{:S(2)}) copy-start(bf16[8,96,2048]{2,1,0:T(8,128)(2,1)} %all-gather.6.cloned.1.call-done) | copy-start | bytes 9437188
  236.6 5.6 %copy-start.4 = (f32[192,2]{0,1:T(2,128)S(1)}, f32[192,2]{0,1:T(2,128)}, u32[]{:S(2)}) copy-start(f32[192,2]{0,1:T(2,128)} %param.29) | copy-start | bytes 4612
  236.6 26.2 %all-to-all-start.1 = ((bf16[8,96,512]{2,1,0:T(8,128)(2,1)}), bf16[8,96,512]{2,1,0:T(8,128)(2,1)S(1)}, u32[]{:S(2)}, u32[]{:S(2)}) async-start(bf16[8,96,512]{2,1,0:T(8,128)(2,1)} %bitcast.65), calls=%async_computation.1 | async-start | bytes 1572864 | tf_op jit(solution)/shard_map/all_to_all | solution.py:155
Sparse Core Ops, SparseCore 0:
  9.5 62.7 all-gather.3
  143.2 26.8 all-gather.5
  181.9 46.3 all-gather.7
